TPU v7x, 256 devices: a whole 4x4x8 slice. The times are simulated.
256 devices in a mesh: sp: 64 (over z, x, core), tp: 4 (over y).
Axes of the slice: x: 4, y: 4, z: 8, core: 2. Of those that a mesh axis runs over, the one named last changes fastest.
Arguments:
- queries: bfloat16 [8192, 2048], P('sp', 'tp'), may hold values from -6 to 6
- key_rows: bfloat16 [8192, 2048], P('sp', 'tp'), may hold values from -6 to 6
- value_rows: bfloat16 [8192, 2048], P('sp', 'tp'), may hold values from -6 to 6
- gate_input: bfloat16 [8192, 2048], P('sp', 'tp'), may hold values from -6 to 6
- log_decay: float32 [8192, 16], P('sp', 'tp'), may hold values from -0.6 to 0, as said below
- head_gain: float32 [2048], P('tp'), may hold values from 0.1 to 1.9
- out_weight: bfloat16 [2048, 2048], P('tp'), may hold values from -0.125 to 0.125
- residual: bfloat16 [8192, 2048], P('sp'), may hold values from -6 to 6
- mlp_gain: float32 [2048], replicated, may hold values from 0.1 to 1.9
- gate_weight: bfloat16 [2048, 5632], P('sp', 'tp'), may hold values from -0.125 to 0.125
- up_weight: bfloat16 [2048, 5632], P('sp', 'tp'), may hold values from -0.125 to 0.125
- down_weight: bfloat16 [5632, 2048], P('tp', 'sp'), may hold values from -0.078125 to 0.078125
Outputs:
- layer_out: bfloat16 [8192, 2048], P(('sp', 'tp'))
Inputs may be any that keep to these rules, and one draw needn't show every extreme that they name: log_decay holds the logarithm of a decay factor of each head at each position.
All inputs are finite; a program needn't handle non-finite values.
Results may differ from a plain program's by a relative error of at most 0.017.
Values may be sent and summed in bfloat16 or wider, within the bound.
A program may use at most 128 MiB of HBM per device.

v0:
```python
import jax
import jax.numpy as jnp
from jax import lax
from jax.sharding import Mesh
from jax.sharding import PartitionSpec as P

BLOCK = 128
SP = ("sp_0", "sp_1", "sp_2")
SP_TP = ("sp_0", "sp_1", "sp_2", "tp")
EPS = 1e-06


def gather_turned(arrays, axis, dims):
    turned = [jnp.moveaxis(a, dim, 0) for a, dim in zip(arrays, dims)]
    widths = [t[0].size for t in turned]
    both = jnp.concatenate([t.reshape(-1, w) for t, w in zip(turned, widths)], axis=1)
    filled = lax.all_gather(both, axis, axis=0, tiled=True)
    blocks = jnp.split(filled, [sum(widths[:k]) for k in range(1, len(widths))], axis=1)
    return tuple(
        (
            jnp.moveaxis(b.reshape(-1, *t.shape[1:]), 0, dim)
            for b, t, dim in zip(blocks, turned, dims)
        )
    )


def nothing_yet(x, identity):
    return jax.tree.map(
        lambda part, zero: jnp.zeros_like(part) + jnp.asarray(zero, part.dtype), x, identity
    )


def carried_in(x, axes, combine, identity):
    before = start = nothing_yet(x, identity)
    total = x
    for axis in reversed(axes):
        length, index = (lax.axis_size(axis), lax.axis_index(axis))
        pieces = jax.tree.map(
            lambda part, kind: lax.all_gather(part.astype(kind), axis),
            total,
            (jnp.bfloat16, jnp.bfloat16),
        )
        inside, total = (start, start)
        for k in range(length):
            passed = k < index
            total = combine(
                total, jax.tree.map(lambda part, own: part[k].astype(own.dtype), pieces, x)
            )
            inside = jax.tree.map(lambda new, old: jnp.where(passed, new, old), total, inside)
        before = combine(inside, before)
    return before


def copy_for_each(x, axis):
    length = lax.axis_size(axis)
    return lax.all_to_all(jnp.broadcast_to(x[None], (length, *x.shape)), axis, 0, 0, tiled=True)


def over_copies(x, axis):
    return copy_for_each(x, axis).astype(jnp.float32).sum(axis=0)


def split_up(x, dim, length):
    dims = x.shape
    blocks = x.reshape(*dims[:dim], length, dims[dim] // length, *dims[dim + 1 :])
    return jnp.moveaxis(blocks, dim, 0)


def sum_at_owner(x, axis, dim):
    blocks = split_up(x, dim, lax.axis_size(axis))
    arrived = lax.all_to_all(blocks, axis, split_axis=0, concat_axis=0, tiled=True)
    return arrived.astype(jnp.float32).sum(axis=0)


def rotate(values_in, positions):
    half = values_in.shape[-1] // 2
    freq = 10000.0 ** (-jnp.linspace(0.0, 1.0, half, dtype=jnp.float32))
    angles = positions * freq
    angles = jnp.concatenate([angles, angles], axis=-1)
    first = values_in[..., :half]
    second = values_in[..., half:]
    turned = jnp.concatenate([-second, first], axis=-1)
    return values_in * jnp.cos(angles) + turned * jnp.sin(angles)


def row_norm(stream, gain):
    return stream * lax.rsqrt(jnp.mean(stream * stream, axis=-1, keepdims=True) + EPS) * gain


def join_states(earlier, later):
    return (earlier[0] * later[0], later[0][:, None, None] * earlier[1] + later[1])


def body(
    queries,
    key_rows,
    value_rows,
    gate_input,
    log_decay,
    head_gain,
    out_weight,
    residual,
    mlp_gain,
    gate_weight,
    up_weight,
    down_weight,
):
    tok_rows = queries.shape[0]
    heads_here = log_decay.shape[1]
    head_size = head_gain.shape[0] // heads_here
    quarter = tok_rows // lax.axis_size("tp")
    full_gate, full_up, full_down = gather_turned(
        (gate_weight, up_weight, down_weight), SP, (0, 0, 1)
    )
    offset = lax.axis_index(SP) * tok_rows
    positions = (offset + lax.iota(jnp.int32, tok_rows)).astype(jnp.float32)[:, None, None]
    q_rot = rotate(
        queries.reshape(tok_rows, heads_here, head_size).astype(jnp.float32), positions
    ).astype(jnp.bfloat16)
    k_rot = (
        rotate(key_rows.reshape(tok_rows, heads_here, head_size).astype(jnp.float32), positions)
        * head_size ** (-0.5)
    ).astype(jnp.bfloat16)
    blocks = tok_rows // BLOCK
    q_blocks = q_rot.reshape(blocks, BLOCK, heads_here, head_size)
    k_blocks = k_rot.reshape(blocks, BLOCK, heads_here, head_size)
    v_blocks = value_rows.reshape(blocks, BLOCK, heads_here, head_size)
    cumul = jnp.cumsum(log_decay.reshape(blocks, BLOCK, heads_here), axis=1)
    by_head = cumul.transpose(0, 2, 1)
    lower = jnp.tril(jnp.ones((BLOCK, BLOCK), dtype=bool))
    spread = by_head[:, :, :, None] - by_head[:, :, None, :]
    weight = jnp.where(lower, jnp.exp(jnp.where(lower, spread, 0.0)), 0.0)
    scores = jnp.einsum("nthd,nshd->nhts", q_blocks, k_blocks, preferred_element_type=jnp.float32)
    probs = (scores * weight).astype(jnp.bfloat16)
    inner = jnp.einsum("nhts,nshe->nthe", probs, v_blocks, preferred_element_type=jnp.float32)
    k_weighted = (
        k_blocks.astype(jnp.float32) * jnp.exp(cumul[:, -1:, :] - cumul)[..., None]
    ).astype(jnp.bfloat16)
    contrib = jnp.einsum(
        "nshd,nshe->nhde", k_weighted, v_blocks, preferred_element_type=jnp.float32
    )
    totals = jnp.exp(cumul[:, -1, :])

    def advance(carry, items):
        state, prefix = carry
        factor, update = items
        return ((state * factor[:, None, None] + update, prefix * factor), (state, prefix))

    start_state = jnp.zeros((heads_here, head_size, head_size), jnp.float32)
    start_prefix = jnp.ones((heads_here,), jnp.float32)
    (dev_state, dev_total), (local_before, prefixes) = lax.scan(
        advance, (start_state, start_prefix), (totals, contrib)
    )
    _, incoming = carried_in((dev_total, dev_state), SP, join_states, (start_prefix, start_state))
    before = local_before + prefixes[:, :, None, None] * incoming[None]
    cross = jnp.einsum(
        "nthd,nhde->nthe", q_blocks.astype(jnp.float32), before, precision=lax.Precision.HIGHEST
    )
    cross = cross * jnp.exp(cumul)[..., None]
    result = (inner + cross).reshape(tok_rows, heads_here, head_size)
    result = row_norm(result, head_gain.reshape(heads_here, head_size)).reshape(
        tok_rows, heads_here * head_size
    )
    retained = (result * jax.nn.silu(gate_input.astype(jnp.float32))).astype(jnp.bfloat16)
    partial_value = jnp.dot(retained, out_weight, preferred_element_type=jnp.float32)
    mixed = over_copies(partial_value.astype(jnp.bfloat16), "tp").astype(jnp.float32)
    middle = (residual.astype(jnp.float32) + mixed).astype(jnp.bfloat16)
    normed = row_norm(middle.astype(jnp.float32), mlp_gain).astype(jnp.bfloat16)
    rows_mid = lax.dynamic_slice_in_dim(middle, lax.axis_index("tp") * quarter, quarter, 0)
    gate = jnp.dot(normed, full_gate, preferred_element_type=jnp.float32)
    upvals = jnp.dot(normed, full_up, preferred_element_type=jnp.float32)
    hidden = (jax.nn.silu(gate) * upvals).astype(jnp.bfloat16)
    ffn = sum_at_owner(
        jnp.dot(hidden, full_down, preferred_element_type=jnp.float32).astype(jnp.bfloat16), "tp", 0
    )
    return (rows_mid.astype(jnp.float32) + ffn).astype(jnp.bfloat16)


def solution(mesh):
    finer = Mesh(mesh.devices.reshape(8, 4, 2, mesh.shape["tp"]), ("sp_0", "sp_1", "sp_2", "tp"))
    in_specs = (
        P(SP, "tp"),
        P(SP, "tp"),
        P(SP, "tp"),
        P(SP, "tp"),
        P(SP, "tp"),
        P("tp"),
        P("tp", None),
        P(SP, None),
        P(),
        P(SP, "tp"),
        P(SP, "tp"),
        P("tp", SP),
    )
    out_specs = P(SP_TP, None)
    return jax.shard_map(body, mesh=finer, in_specs=in_specs, out_specs=out_specs, check_vma=False)
```

profile of v0, /device:TPU:1, one launch (start us, length us, event | category | flops | bytes accessed | tf_op | source)
XLA Modules:
  0.0 215.4 jit_solution(10362698421659114462)
XLA Ops:
  6.5 0.0 copy-start
  6.5 0.0 all-gather.7.cloned.1.call-start
  6.6 0.9 copy.69
  7.5 0.2 reduce_window_sum.13
  7.7 0.1 copy.73
  7.8 4.7 %all-gather = bf16[2,1,4]{2,1,0:T(2,128)(2,1)S(1)} all-gather(bf16[1,1,4]{2,1,0:T(2,128)(2,1)S(1)} %get-tuple-element.38), channel_id=2, replica_groups=mesh['sp_0'=8,'sp_1'=4,'sp_2'=2,'tp'=4] {'sp_2'}, dimensions={0}, use_global_device_ids=true | all-gather | bytes 24 | tf_op jit(solution)/shard_map/all_gather | solution.py:39
  12.5 0.1 fusion.162
  12.6 0.1 broadcast_multiply_fusion
  12.7 0.3 fusion.150
  13.0 0.9 copy_bitcast_fusion
  13.9 0.9 copy_bitcast_fusion.1
  14.8 0.2 slice_negate_fusion
  15.0 0.1 bitcast_exponential_fusion
  15.1 1.2 fusion.39
  16.3 1.2 fusion.20
  17.6 2.0 all-gather.1
  19.6 6.0 %all-gather.2 = bf16[4,1,4]{2,1,0:T(2,128)(2,1)S(1)} all-gather(bf16[1,1,4]{2,1,0:T(2,128)(2,1)S(1)} %multiply_convert_fusion.2), channel_id=1, replica_groups=mesh['sp_0'=8,'sp_1'=4,'sp_2'=2,'tp'=4] {'sp_1'}, dimensions={0}, use_global_device_ids=true | all-gather | bytes 40 | tf_op jit(solution)/shard_map/all_gather | solution.py:39
  25.6 0.1 fusion.90
  25.7 11.4 %all_gather.31 = bf16[4,4,128,128]{3,2,1,0:T(8,128)(2,1)S(1)} all-gather(bf16[1,4,128,128]{3,2,1,0:T(8,128)(2,1)S(1)} %fusion.90), channel_id=1, replica_groups=mesh['sp_0'=8,'sp_1'=4,'sp_2'=2,'tp'=4] {'sp_1'}, dimensions={0}, use_global_device_ids=true | all-gather | bytes 655360 | tf_op jit(solution)/shard_map/all_gather | solution.py:39
  37.0 0.8 fusion.84
  37.9 0.0 all-gather.7.cloned.1.call-update
  37.9 0.0 all-gather.9.cloned.1.call-start
  37.9 0.0 copy-done.2
  38.0 0.7 pad_maximum_fusion
  38.7 0.0 all-gather.9.cloned.1.call-update
  38.7 14.3 %all-gather.3 = bf16[8,1,4]{2,1,0:T(2,128)(2,1)S(1)} all-gather(bf16[1,1,4]{2,1,0:T(2,128)(2,1)S(1)} %fusion.164), channel_id=1, replica_groups=mesh['sp_0'=8,'sp_1'=4,'sp_2'=2,'tp'=4] {'sp_0'}, dimensions={0}, use_global_device_ids=true | all-gather | bytes 72 | tf_op jit(solution)/shard_map/all_gather | solution.py:39
  53.0 0.1 copy.70
  53.1 2.0 convolution_bitcast_fusion.1
  55.1 20.8 %all-gather.7.cloned.1.call-done = bf16[8,4,128,128]{3,2,1,0:T(8,128)(2,1)} async-done(((bf16[1,4,128,128]{3,2,1,0:T(8,128)(2,1)}), bf16[8,4,128,128]{3,2,1,0:T(8,128)(2,1)}) %all-gather.7.cloned.1.call-update) | async-done | bytes 1048592 | tf_op jit(solution)/shard_map/all_gather | solution.py:39
  76.0 2.3 %multiply_reduce_fusion = (f32[128,4]{0,1:T(4,128)S(1)}, f32[1,128,4,128]{1,3,2,0:T(8,128)S(1)}) fusion(f32[1,128,4,128]{1,3,2,0:T(8,128)} %convolution_bitcast_fusion.1, f32[128,4]{0,1:T(4,128)S(1)} %get-tuple-element.49, bf16[128,4,128]{2,0,1:T(8,128)(2,1)S(1)} %get-tuple-element.36, bf16[8,4,128,128]{3,2,1,0:T(8,128)(2,1)} %all-gather.7.cloned.1.call-done, ...), kind=kOutput, calls=%fused_computation.63 | convolution fusion | flops 104660480 | bytes 2494734 | tf_op jit(solution)/shard_map/nthd,nhde->nthe/dot_general | solution.py:156
  78.3 0.1 copy.77
  78.4 0.1 copy.78
  78.6 0.2 mul.480
  78.8 0.5 convolution_convert_fusion
  79.3 0.0 copy-start.1
  79.3 0.0 copy-start.6
  79.3 0.2 broadcast_in_dim.36
  79.6 24.2 %all_to_all.10 = bf16[4,128,2048]{2,1,0:T(8,128)(2,1)S(1)} all-to-all(bf16[4,128,2048]{2,1,0:T(8,128)(2,1)S(1)} %broadcast_in_dim.36), channel_id=1, replica_groups=mesh['sp_0'=8,'sp_1'=4,'sp_2'=2,'tp'=4] {'tp'}, dimensions={0} | all-to-all | bytes 4194304 | tf_op jit(solution)/shard_map/all_to_all | solution.py:56
  103.8 0.4 convert_reduce_fusion
  104.2 0.0 copy-done.1
  104.2 0.2 fusion.21
  104.4 78.6 %all-gather.9.cloned.1.call-done = bf16[2048,4224]{1,0:T(8,128)(2,1)} async-done(((bf16[32,4224]{1,0:T(8,128)(2,1)}), bf16[2048,4224]{1,0:T(8,128)(2,1)}) %all-gather.9.cloned.1.call-update) | async-done | bytes 17301520 | tf_op jit(solution)/shard_map/all_gather | solution.py:17
  183.0 3.7 %fusion.4 = f32[128,1408]{1,0:T(8,128)S(1)} fusion(bf16[2048,4224]{1,0:T(8,128)(2,1)} %all-gather.9.cloned.1.call-done, bf16[128,2048]{1,0:T(8,128)(2,1)S(1)} %get-tuple-element.19, f32[2048]{0:T(1024)S(1)} %copy-done.6, f32[128]{0:T(128)S(1)} %add_rsqrt_fusion.1), kind=kOutput, calls=%fused_computation.4 | convolution fusion | flops 739246080 | bytes 7021056 | tf_op jit(solution)/shard_map/dot_general | solution.py:170
  186.7 8.0 %fusion.9 = bf16[128,2048]{1,0:T(8,128)(2,1)} fusion(bf16[2048,4224]{1,0:T(8,128)(2,1)} %all-gather.9.cloned.1.call-done, f32[128,1408]{1,0:T(8,128)S(1)} %fusion.4, bf16[128,2048]{1,0:T(8,128)(2,1)S(1)} %get-tuple-element.19, f32[2048]{0:T(1024)S(1)} %copy-done.6, f32[128]{0:T(128)S(1)} %add_rsqrt_fusion.1), kind=kOutput, calls=%fused_computation.8 | convolution fusion | flops 1478787072 | bytes 13312512 | tf_op jit(solution)/shard_map/dot_general | solution.py:174
  194.7 4.0 %all-to-all-start.1 = ((bf16[4,32,2048]{2,1,0:T(8,128)(2,1)}), bf16[4,32,2048]{2,1,0:T(8,128)(2,1)S(1)}, u32[]{:S(2)}, u32[]{:S(2)}) async-start(bf16[4,32,2048]{2,1,0:T(8,128)(2,1)} %bitcast.176), calls=%async_computation.1 | async-start | bytes 1048576 | tf_op jit(solution)/shard_map/all_to_all | solution.py:71
  198.7 9.0 %all-to-all-done.1 = bf16[4,32,2048]{2,1,0:T(8,128)(2,1)S(1)} async-done(((bf16[4,32,2048]{2,1,0:T(8,128)(2,1)}), bf16[4,32,2048]{2,1,0:T(8,128)(2,1)S(1)}, u32[]{:S(2)}, u32[]{:S(2)}) %all-to-all-start.1) | async-done | bytes 524320 | tf_op jit(solution)/shard_map/all_to_all | solution.py:71
  207.8 0.1 convert_reduce_fusion.1
  207.8 0.7 add_convert_fusion.1
  (25 shorter events, 0.1 us)
Async XLA Ops:
  6.5 72.2 %copy-start = (bf16[512,2048]{1,0:T(8,128)(2,1)S(1)}, bf16[512,2048]{1,0:T(8,128)(2,1)}, u32[]{:S(2)}) copy-start(bf16[512,2048]{1,0:T(8,128)(2,1)} %param.20) | copy-start | bytes 6291460
  6.5 31.4 %copy-start.2 = (bf16[1408,32]{0,1:T(8,128)(2,1)S(1)}, bf16[1408,32]{0,1:T(8,128)(2,1)}, u32[]{:S(2)}) copy-start(bf16[1408,32]{0,1:T(8,128)(2,1)} %param.25) | copy-start | bytes 270340
  6.5 31.4 %copy-start.4 = (bf16[32,1408]{1,0:T(8,128)(2,1)S(1)}, bf16[32,1408]{1,0:T(8,128)(2,1)}, u32[]{:S(2)}) copy-start(bf16[32,1408]{1,0:T(8,128)(2,1)} %param.23) | copy-start | bytes 270340
  6.5 31.4 %copy-start.3 = (bf16[32,1408]{1,0:T(8,128)(2,1)S(1)}, bf16[32,1408]{1,0:T(8,128)(2,1)}, u32[]{:S(2)}) copy-start(bf16[32,1408]{1,0:T(8,128)(2,1)} %param.24) | copy-start | bytes 270340
  6.5 69.4 %all-gather.7.cloned.1.call-start = ((), (), s32[]{:S(2)}) async-start(), calls=%async_computation.2 | async-start | bytes 1179648 | tf_op jit(solution)/shard_map/all_gather | solution.py:39
  15.1 63.7 %copy-start.7 = (f32[512]{0:T(512)S(1)}, f32[512]{0:T(512)}, u32[]{:S(2)}) copy-start(f32[512]{0:T(512)} %param.19) | copy-start | bytes 6148
  37.9 145.1 %all-gather.9.cloned.1.call-start = ((), (), s32[]{:S(2)}) async-start(), calls=%async_computation.3 | async-start | bytes 17571840 | tf_op jit(solution)/shard_map/all_gather | solution.py:17
  55.1 23.7 %copy-start.5 = (bf16[128,512]{1,0:T(8,128)(2,1)S(1)}, bf16[128,512]{1,0:T(8,128)(2,1)}, u32[]{:S(2)}) copy-start(bf16[128,512]{1,0:T(8,128)(2,1)} %param.17) | copy-start | bytes 393220
  79.3 24.9 %copy-start.1 = (bf16[128,2048]{1,0:T(8,128)(2,1)S(1)}, bf16[128,2048]{1,0:T(8,128)(2,1)}, u32[]{:S(2)}) copy-start(bf16[128,2048]{1,0:T(8,128)(2,1)} %param.21) | copy-start | bytes 1572868
  79.3 103.7 %copy-start.6 = (f32[2048]{0:T(1024)S(1)}, f32[2048]{0:T(1024)}, u32[]{:S(2)}) copy-start(f32[2048]{0:T(1024)} %param.22) | copy-start | bytes 24580
  194.7 13.0 %all-to-all-start.1 = ((bf16[4,32,2048]{2,1,0:T(8,128)(2,1)}), bf16[4,32,2048]{2,1,0:T(8,128)(2,1)S(1)}, u32[]{:S(2)}, u32[]{:S(2)}) async-start(bf16[4,32,2048]{2,1,0:T(8,128)(2,1)} %bitcast.176), calls=%async_computation.1 | async-start | bytes 1048576 | tf_op jit(solution)/shard_map/all_to_all | solution.py:71
Sparse Core Ops, SparseCore 0:
  38.0 37.9 all-gather.6
  78.7 104.2 all-gather.8
where the time goes:
time: 216 us; the launch traced here: 215 us
  waiting for transfers between devices  108 us (50%)
  blocking collectives  62.5 us (29%)
  matrix products  17.7 us (8%)
  between operations  13.6 us (6%)
  other arithmetic  7.15 us (3%)
  starting transfers between devices  4.07 us (2%)
    all_gather x1, waiting for transfers between devices, gather_turned(): filled = lax.all_gather(both, axis, axis=0, tiled=True)  78.6 us
    all_gather x5, blocking collectives, carried_in(): lax.all_gather(part.astype(kind), axis)  38.3 us
    all_to_all x1, blocking collectives, copy_for_each(): lax.all_to_all(jnp.broadcast_to(x[None], (length, *x.shape)), axis, 0, 0,...  24.2 us
    all_gather x1, waiting for transfers between devices, carried_in(): lax.all_gather(part.astype(kind), axis)  20.8 us
    all_to_all x1, waiting for transfers between devices, sum_at_owner(): lax.all_to_all(blocks, axis, split_axis=0, concat_axis=0, tiled=True)  9.03 us
    dot_general x1, matrix products, body(): jnp.dot(hidden, full_down, preferred_element_type=jnp.float32)  8.02 us
  transfers between devices with their start and end apart: 3, of which 3 were waited for; matrix products, arithmetic and copies ran while one was open for 3% of the time, Pallas kernels for 0%

commit v1 on v0

--- a/solution.py
+++ b/solution.py
@@ -14,7 +14,9 @@
     turned = [jnp.moveaxis(a, dim, 0) for a, dim in zip(arrays, dims)]
     widths = [t[0].size for t in turned]
     both = jnp.concatenate([t.reshape(-1, w) for t, w in zip(turned, widths)], axis=1)
-    filled = lax.all_gather(both, axis, axis=0, tiled=True)
+    filled = jnp.concatenate(
+        lax.all_to_all(jnp.stack([both] * lax.axis_size(axis)), axis, 0, 0), axis=0
+    )
     blocks = jnp.split(filled, [sum(widths[:k]) for k in range(1, len(widths))], axis=1)
     return tuple(
         (

time: 216 us -> 545 us (2.52); the launches traced: 215 us -> 536 us
  waiting for transfers between devices: 108 us -> 424 us
  blocking collectives: 62.5 us -> 39.9 us
  starting transfers between devices: 4.07 us -> 22.8 us
  local copies, waits for them, and re-layouts: 1.78 us -> 9.27 us
    all_to_all x0 -> x2, waiting for transfers between devices: none -> 395 us  [the longest x1 374 us: gather_turned(): lax.all_to_all(jnp.stack([both] * lax.axis_size(axis)), axis, 0, 0)]
    all_gather x1 -> x0, waiting for transfers between devices: 78.6 us -> none  [gather_turned(): filled = lax.all_gather(both, axis, axis=0, tiled=True)]
    all_to_all x1 -> x0, blocking collectives: 24.2 us -> none  [copy_for_each(): lax.all_to_all(jnp.broadcast_to(x[None], (length, *x.shape)), axis, 0, 0,...]
    all_to_all x0 -> x2, starting transfers between devices: none -> 19.3 us  [the longest x1 14.9 us: gather_turned(): lax.all_to_all(jnp.stack([both] * lax.axis_size(axis)), axis, 0, 0)]
    another operation x0 -> x1, local copies, waits for them, and re-layouts: none -> 6.1 us  [gather_turned(): jnp.stack([both] * lax.axis_size(axis))]
  transfers between devices with their start and end apart: 3 -> 4, of which waited for: 3 -> 4; matrix products, arithmetic and copies ran while one was open for 3% -> 1% of each run, Pallas kernels for 0% -> 0%
where the time goes in v1:
time: 545 us; the launch traced here: 536 us
  waiting for transfers between devices  424 us (78%)
  blocking collectives  39.9 us (7%)
  starting transfers between devices  22.8 us (4%)
  matrix products  17.9 us (3%)
  between operations  13.7 us (3%)
  local copies, waits for them, and re-layouts  9.27 us (2%)
  other arithmetic  8.17 us (1%)
    all_to_all x1, waiting for transfers between devices, gather_turned(): lax.all_to_all(jnp.stack([both] * lax.axis_size(axis)), axis, 0, 0)  374 us
    all_gather x5, blocking collectives, carried_in(): lax.all_gather(part.astype(kind), axis)  39.9 us
    all_gather x1, waiting for transfers between devices, carried_in(): lax.all_gather(part.astype(kind), axis)  21.5 us
    all_to_all x1, waiting for transfers between devices, copy_for_each(): lax.all_to_all(jnp.broadcast_to(x[None], (length, *x.shape)), axis, 0, 0,...  20.4 us
    all_to_all x1, starting transfers between devices, gather_turned(): lax.all_to_all(jnp.stack([both] * lax.axis_size(axis)), axis, 0, 0)  14.9 us
  transfers between devices with their start and end apart: 4, of which 4 were waited for; matrix products, arithmetic and copies ran while one was open for 1% of the time, Pallas kernels for 0%

profile of v1, /device:TPU:1, one launch (start us, length us, event | category | flops | bytes accessed | tf_op | source)
XLA Modules:
  0.0 535.6 jit_solution(16057579667690061415)
XLA Ops:
  6.5 0.0 copy-start
  6.6 1.0 copy.69
  7.5 0.2 reduce_window_sum.13
  7.7 0.1 copy.73
  7.8 4.7 all-gather
  12.5 0.9 copy_bitcast_fusion
  13.4 0.9 copy_bitcast_fusion.1
  14.3 0.1 fusion.162
  14.4 0.1 broadcast_multiply_fusion
  14.5 0.3 fusion.150
  14.8 6.0 %all-gather.2 = bf16[4,1,4]{2,1,0:T(2,128)(2,1)S(1)} all-gather(bf16[1,1,4]{2,1,0:T(2,128)(2,1)S(1)} %multiply_convert_fusion.2), channel_id=1, replica_groups=mesh['sp_0'=8,'sp_1'=4,'sp_2'=2,'tp'=4] {'sp_1'}, dimensions={0}, use_global_device_ids=true | all-gather | bytes 40 | tf_op jit(solution)/shard_map/all_gather | solution.py:41
  20.8 0.2 slice_negate_fusion
  21.1 0.0 copy-start.6
  21.1 0.0 copy-start.8
  21.1 0.1 bitcast_exponential_fusion
  21.1 1.2 fusion.39
  22.3 1.2 fusion.20
  23.6 4.0 all-gather.1
  27.6 0.1 fusion.90
  27.7 9.9 %all_gather.28 = bf16[4,4,128,128]{3,2,1,0:T(8,128)(2,1)S(1)} all-gather(bf16[1,4,128,128]{3,2,1,0:T(8,128)(2,1)S(1)} %fusion.90), channel_id=1, replica_groups=mesh['sp_0'=8,'sp_1'=4,'sp_2'=2,'tp'=4] {'sp_1'}, dimensions={0}, use_global_device_ids=true | all-gather | bytes 655360 | tf_op jit(solution)/shard_map/all_gather | solution.py:41
  37.6 0.8 fusion.84
  38.4 0.0 all-gather.6.cloned.1.call-update
  38.5 15.4 %all-gather.3 = bf16[8,1,4]{2,1,0:T(2,128)(2,1)S(1)} all-gather(bf16[1,1,4]{2,1,0:T(2,128)(2,1)S(1)} %fusion.164), channel_id=1, replica_groups=mesh['sp_0'=8,'sp_1'=4,'sp_2'=2,'tp'=4] {'sp_0'}, dimensions={0}, use_global_device_ids=true | all-gather | bytes 72 | tf_op jit(solution)/shard_map/all_gather | solution.py:41
  53.9 0.1 copy.70
  54.0 1.1 convolution_bitcast_fusion.1
  55.1 21.5 %all-gather.6.cloned.1.call-done = bf16[8,4,128,128]{3,2,1,0:T(8,128)(2,1)} async-done(((bf16[1,4,128,128]{3,2,1,0:T(8,128)(2,1)}), bf16[8,4,128,128]{3,2,1,0:T(8,128)(2,1)}) %all-gather.6.cloned.1.call-update) | async-done | bytes 1048592 | tf_op jit(solution)/shard_map/all_gather | solution.py:41
  76.6 2.4 multiply_reduce_fusion
  79.0 0.0 copy-start.2
  79.0 0.0 copy-start.3
  79.0 0.0 copy-start.4
  79.0 0.1 copy.78
  79.1 0.1 copy.77
  79.3 0.2 mul.480
  79.5 0.5 convolution_convert_fusion
  80.0 1.6 broadcast_in_dim.36
  81.6 4.5 all-to-all-start
  86.1 20.4 %all-to-all-done = bf16[4,128,2048]{2,1,0:T(8,128)(2,1)} async-done(((bf16[4,128,2048]{2,1,0:T(8,128)(2,1)}), bf16[4,128,2048]{2,1,0:T(8,128)(2,1)}, u32[]{:S(2)}, u32[]{:S(2)}) %all-to-all-start) | async-done | bytes 2097184 | tf_op jit(solution)/shard_map/all_to_all | solution.py:58
  106.5 6.1 %stack.2 = bf16[64,32,4224]{2,1,0:T(8,128)(2,1)} broadcast(bf16[32,4224]{1,0:T(8,128)(2,1)S(1)} %pad_maximum_fusion), dimensions={1,2} | broadcast | bytes 17571840 | tf_op jit(solution)/shard_map/stack | solution.py:18
  112.6 14.9 %all-to-all-start.1 = ((bf16[64,32,4224]{2,1,0:T(8,128)(2,1)}), bf16[64,32,4224]{2,1,0:T(8,128)(2,1)}, u32[]{:S(2)}, u32[]{:S(2)}) async-start(bf16[64,32,4224]{2,1,0:T(8,128)(2,1)} %stack.2), calls=%async_computation.1 | async-start | bytes 34603008 | tf_op jit(solution)/shard_map/all_to_all | solution.py:18
  127.5 2.1 convert_reduce_fusion
  129.6 0.3 fusion.21
  129.9 374.1 %all-to-all-done.1 = bf16[64,32,4224]{2,1,0:T(8,128)(2,1)} async-done(((bf16[64,32,4224]{2,1,0:T(8,128)(2,1)}), bf16[64,32,4224]{2,1,0:T(8,128)(2,1)}, u32[]{:S(2)}, u32[]{:S(2)}) %all-to-all-start.1) | async-done | bytes 17301536 | tf_op jit(solution)/shard_map/all_to_all | solution.py:18
  504.0 4.5 fusion.4
  508.5 8.2 %fusion.9 = bf16[128,2048]{1,0:T(8,128)(2,1)} fusion(bf16[2048,4224]{1,0:T(8,128)(2,1)} %bitcast.34, f32[128,1408]{1,0:T(8,128)} %fusion.4, bf16[128,2048]{1,0:T(8,128)(2,1)S(1)} %get-tuple-element.19, f32[2048]{0:T(1024)S(1)} %copy-done.7, f32[128]{0:T(128)S(1)} %add_rsqrt_fusion.1), kind=kOutput, calls=%fused_computation.8 | convolution fusion | flops 1478787072 | bytes 13312512 | tf_op jit(solution)/shard_map/dot_general | solution.py:176
  516.7 3.5 all-to-all-start.2
  520.2 7.8 %all-to-all-done.2 = bf16[4,32,2048]{2,1,0:T(8,128)(2,1)S(1)} async-done(((bf16[4,32,2048]{2,1,0:T(8,128)(2,1)}), bf16[4,32,2048]{2,1,0:T(8,128)(2,1)S(1)}, u32[]{:S(2)}, u32[]{:S(2)}) %all-to-all-start.2) | async-done | bytes 524320 | tf_op jit(solution)/shard_map/all_to_all | solution.py:73
  528.0 0.1 convert_reduce_fusion.1
  528.1 0.7 add_convert_fusion.1
  (28 shorter events, 0.2 us)
Async XLA Ops:
  6.5 72.9 %copy-start = (bf16[512,2048]{1,0:T(8,128)(2,1)S(1)}, bf16[512,2048]{1,0:T(8,128)(2,1)}, u32[]{:S(2)}) copy-start(bf16[512,2048]{1,0:T(8,128)(2,1)} %param.20) | copy-start | bytes 6291460
  6.5 47.4 %copy-start.5 = (bf16[128,512]{1,0:T(8,128)(2,1)S(1)}, bf16[128,512]{1,0:T(8,128)(2,1)}, u32[]{:S(2)}) copy-start(bf16[128,512]{1,0:T(8,128)(2,1)} %param.16) | copy-start | bytes 393220
  6.5 70.1 %all-gather.6.cloned.1.call-start = ((), (), s32[]{:S(2)}) async-start(), calls=%async_computation.3 | async-start | bytes 1179648 | tf_op jit(solution)/shard_map/all_gather | solution.py:41
  21.1 58.4 %copy-start.6 = (bf16[128,512]{1,0:T(8,128)(2,1)S(1)}, bf16[128,512]{1,0:T(8,128)(2,1)}, u32[]{:S(2)}) copy-start(bf16[128,512]{1,0:T(8,128)(2,1)} %param.17) | copy-start | bytes 393220
  21.1 58.4 %copy-start.8 = (f32[512]{0:T(512)S(1)}, f32[512]{0:T(512)}, u32[]{:S(2)}) copy-start(f32[512]{0:T(512)} %param.19) | copy-start | bytes 6148
  79.0 7.1 %copy-start.2 = (bf16[1408,32]{0,1:T(8,128)(2,1)S(1)}, bf16[1408,32]{0,1:T(8,128)(2,1)}, u32[]{:S(2)}) copy-start(bf16[1408,32]{0,1:T(8,128)(2,1)} %param.25) | copy-start | bytes 270340
  79.0 7.1 %copy-start.3 = (bf16[32,1408]{1,0:T(8,128)(2,1)S(1)}, bf16[32,1408]{1,0:T(8,128)(2,1)}, u32[]{:S(2)}) copy-start(bf16[32,1408]{1,0:T(8,128)(2,1)} %param.24) | copy-start | bytes 270340
  79.0 7.1 %copy-start.4 = (bf16[32,1408]{1,0:T(8,128)(2,1)S(1)}, bf16[32,1408]{1,0:T(8,128)(2,1)}, u32[]{:S(2)}) copy-start(bf16[32,1408]{1,0:T(8,128)(2,1)} %param.23) | copy-start | bytes 270340
  81.6 25.0 %all-to-all-start = ((bf16[4,128,2048]{2,1,0:T(8,128)(2,1)}), bf16[4,128,2048]{2,1,0:T(8,128)(2,1)}, u32[]{:S(2)}, u32[]{:S(2)}) async-start(bf16[4,128,2048]{2,1,0:T(8,128)(2,1)} %broadcast_in_dim.36), calls=%async_computation | async-start | bytes 4194304 | tf_op jit(solution)/shard_map/all_to_all | solution.py:58
  112.6 17.0 %copy-start.1 = (bf16[128,2048]{1,0:T(8,128)(2,1)S(1)}, bf16[128,2048]{1,0:T(8,128)(2,1)}, u32[]{:S(2)}) copy-start(bf16[128,2048]{1,0:T(8,128)(2,1)} %param.21) | copy-start | bytes 1572868
  112.6 391.3 %copy-start.7 = (f32[2048]{0:T(1024)S(1)}, f32[2048]{0:T(1024)}, u32[]{:S(2)}) copy-start(f32[2048]{0:T(1024)} %param.22) | copy-start | bytes 24580
  112.6 391.3 %all-to-all-start.1 = ((bf16[64,32,4224]{2,1,0:T(8,128)(2,1)}), bf16[64,32,4224]{2,1,0:T(8,128)(2,1)}, u32[]{:S(2)}, u32[]{:S(2)}) async-start(bf16[64,32,4224]{2,1,0:T(8,128)(2,1)} %stack.2), calls=%async_computation.1 | async-start | bytes 34603008 | tf_op jit(solution)/shard_map/all_to_all | solution.py:18
  516.7 11.3 %all-to-all-start.2 = ((bf16[4,32,2048]{2,1,0:T(8,128)(2,1)}), bf16[4,32,2048]{2,1,0:T(8,128)(2,1)S(1)}, u32[]{:S(2)}, u32[]{:S(2)}) async-start(bf16[4,32,2048]{2,1,0:T(8,128)(2,1)} %bitcast.177), calls=%async_computation.2 | async-start | bytes 1048576 | tf_op jit(solution)/shard_map/all_to_all | solution.py:73
Sparse Core Ops, SparseCore 0:
  38.6 37.9 all-gather.5
